TPU v7x, 32 devices: a whole 2x2x4 slice. The times are simulated.
32 devices in a mesh: grp: 2 (over y), ep: 4 (over z), tp: 4 (over x, core).
Axes of the slice: x: 2, y: 2, z: 4, core: 2. Of those that a mesh axis runs over, the one named last changes fastest.
Arguments:
- tokens: bfloat16 [512, 4096], P(('grp', 'ep'), 'tp'), parts along dimension 0, may hold values from -27 to 27
- group_choice: int32 [512], P(('grp', 'ep')), parts along dimension 0, may hold values from 0 to 1, as said below
- member_choice: int32 [512, 2], P(('grp', 'ep')), parts along dimension 0, may hold values from 0 to 1, as said below
- group_prob: float32 [512], P(('grp', 'ep')), parts along dimension 0, may hold values from 0.3 to 1
- member_score: float32 [512, 2], P(('grp', 'ep')), parts along dimension 0, may hold values from -4 to 4
- norm_gain: float32 [4096], P('tp'), may hold values from 0.1 to 1.9
- w_gate: bfloat16 [4, 4096, 1024], P('ep', 'tp'), may hold values from -0.09375 to 0.09375
- w_up: bfloat16 [4, 4096, 1024], P('ep', 'tp'), may hold values from -0.09375 to 0.09375
- w_down: bfloat16 [4, 1024, 4096], P('ep', None, 'tp'), may hold values from -0.1875 to 0.1875
- final_gain: float32 [4096], P('tp'), may hold values from 0.1 to 1.9
Outputs:
- mixed: bfloat16 [512, 4096], P(('grp', 'ep'), 'tp'), parts along dimension 0
There are 2 independent parts, one for each index of `grp`. A program takes and returns all parts, laid end to end along the dimension named above; an argument that names none is the same for every part. Nothing has to cross between parts.
Inputs may be any that keep to these rules, and one draw needn't show every extreme that they name: `group_choice`: in each aligned block of 64 tokens every group is chosen by exactly 32 tokens. `member_choice`: each row names 2 different experts of its token's group. In each aligned block of 64 rows no expert (group and member together) is named by more than 32 rows, some expert is named by exactly 32 rows, and one expert is named by exactly 32 rows in every block.
All inputs are finite; a program needn't handle non-finite values.
Results may differ from a plain program's by a relative error of at most 0.017.
Values may be sent and summed in bfloat16 or wider, within the bound.
A program may use at most 64 MiB of HBM per device.

v0:
```python
import jax
import jax.numpy as jnp
from jax import lax
from jax.sharding import PartitionSpec as P

EPS = 1e-06


def slot_table(expert_ids, experts, capacity):
    flat_ids = expert_ids.reshape(-1)
    onehot = (flat_ids[:, None] == jnp.arange(experts, dtype=jnp.int32)[None, :]).astype(jnp.int32)
    before = jnp.cumsum(onehot, axis=0) - onehot
    position = jnp.sum(before * onehot, axis=1)
    return (flat_ids * capacity + position).reshape(expert_ids.shape)


def expert_rows(rows_in, gate_w, up_w, down_w):
    gate_part = jnp.dot(rows_in, gate_w, preferred_element_type=jnp.float32)
    up_part = jnp.dot(rows_in, up_w, preferred_element_type=jnp.float32)
    gate_sum, up_sum = (
        lax.psum(gate_part.astype(jnp.bfloat16), "tp").astype(jnp.float32),
        lax.psum(up_part.astype(jnp.bfloat16), "tp").astype(jnp.float32),
    )
    hidden = (jax.nn.silu(gate_sum) * up_sum).astype(jnp.bfloat16)
    return jnp.dot(hidden, down_w, preferred_element_type=jnp.float32).astype(jnp.bfloat16)


def local(
    tokens,
    group_choice,
    member_choice,
    group_prob,
    member_score,
    norm_gain,
    w_gate,
    w_up,
    w_down,
    final_gain,
):
    experts = lax.axis_size("ep")
    groups = max(2, experts // 8)
    per_group = experts // groups
    tok_dev = tokens.shape[0]
    capacity = tok_dev // groups
    full_width = tokens.shape[1] * lax.axis_size("tp")
    gate_w = w_gate[0]
    up_w = w_up[0]
    down_w = w_down[0]
    values = tokens.astype(jnp.float32)
    square_in = lax.psum(jnp.sum(values * values, axis=1), "tp")
    normed = (
        values * lax.rsqrt(square_in[:, None] / full_width + EPS) * norm_gain[None, :]
    ).astype(jnp.bfloat16)
    expert_ids = group_choice[:, None] * per_group + member_choice
    scores = jnp.exp(member_score)
    weights = group_prob[:, None] * scores / jnp.sum(scores, axis=1, keepdims=True)
    destination = slot_table(expert_ids, experts, capacity)
    slot_iota = jnp.arange(experts * capacity, dtype=jnp.int32)
    picker = (destination[:, :, None] == slot_iota[None, None, :]).astype(jnp.bfloat16)
    outgoing = jnp.einsum("tkr,td->rd", picker, normed, preferred_element_type=jnp.float32).astype(
        jnp.bfloat16
    )
    outgoing = outgoing.reshape(experts, capacity, -1)
    received = lax.all_to_all(outgoing, "ep", split_axis=0, concat_axis=0, tiled=True)
    produced = expert_rows(received.reshape(-1, received.shape[2]), gate_w, up_w, down_w)
    returned = lax.all_to_all(
        produced.reshape(received.shape), "ep", split_axis=0, concat_axis=0, tiled=True
    )
    picked_rows = jnp.einsum(
        "tkr,rd->tkd",
        picker,
        returned.reshape(experts * capacity, -1),
        preferred_element_type=jnp.float32,
    )
    moe = jnp.sum(weights[:, :, None] * picked_rows, axis=1)
    summed = values + moe
    square_out = lax.psum(jnp.sum(summed * summed, axis=1), "tp")
    return (
        summed * lax.rsqrt(square_out[:, None] / full_width + EPS) * final_gain[None, :]
    ).astype(jnp.bfloat16)


def solution(mesh):
    return jax.shard_map(
        local,
        mesh=mesh,
        in_specs=(
            P(("grp", "ep"), "tp"),
            P(("grp", "ep")),
            P(("grp", "ep"), None),
            P(("grp", "ep")),
            P(("grp", "ep"), None),
            P("tp"),
            P("ep", "tp", None),
            P("ep", "tp", None),
            P("ep", None, "tp"),
            P("tp"),
        ),
        out_specs=P(("grp", "ep"), "tp"),
        check_vma=False,
    )
```

profile of v0, /device:TPU:0, one launch (start us, length us, event | category | flops | bytes accessed | tf_op | source)
XLA Modules:
  0.0 97.4 jit_solution(12502165521280332977)
XLA Ops:
  6.5 0.8 broadcast_multiply_fusion
  7.3 0.7 broadcast_add_fusion
  8.0 0.1 copy.15
  8.1 0.1 eq.28
  8.3 0.1 fusion.30
  8.4 0.2 reduce_window_sum.11
  8.5 0.2 select_reduce_fusion
  8.7 0.1 reduce_sum.58
  8.9 0.7 multiply_add_fusion
  9.6 0.1 convert_reduce_fusion
  9.7 1.0 %fusion.22 = f32[64]{0:T(128)S(1)} fusion(bf16[64,1024]{1,0:T(8,128)(2,1)} %param.10), kind=kLoop, calls=%fused_computation.22 | loop fusion | flops 196544 | bytes 131328 | tf_op jit(solution)/shard_map/reduce_sum | solution.py:50
  10.8 8.4 %psum.28 = f32[64]{0:T(128)S(1)} all-reduce(f32[64]{0:T(128)S(1)} %fusion.22), channel_id=1, replica_groups=mesh['grp'=2,'ep'=4,'tp'=4] {'tp'}, use_global_device_ids=true, to_apply=%region_5.6 | all-reduce | flops 64 | bytes 512 | tf_op jit(solution)/shard_map/psum | solution.py:50
  19.1 1.3 %convolution_convert_fusion = bf16[128,1024]{1,0:T(8,128)(2,1)S(1)} fusion(bf16[64,128]{1,0:T(8,128)(2,1)S(1)} %convert_reduce_fusion, bf16[64,1024]{1,0:T(8,128)(2,1)} %param.10, f32[1024]{0:T(1024)} %param.15, f32[64]{0:T(128)S(1)} %add_rsqrt_fusion.1), kind=kOutput, calls=%fused_computation.11 | convolution fusion | flops 17039360 | bytes 413952 | tf_op jit(solution)/shard_map/tkr,td->rd/dot_general | solution.py:60
  20.5 12.5 %all_to_all.10 = bf16[4,32,1024]{2,1,0:T(8,128)(2,1)S(1)} all-to-all(bf16[4,32,1024]{2,1,0:T(8,128)(2,1)S(1)} %bitcast.27), channel_id=1, replica_groups=mesh['grp'=2,'ep'=4,'tp'=4] {'ep'}, dimensions={0} | all-to-all | bytes 524288 | tf_op jit(solution)/shard_map/all_to_all | solution.py:64
  33.0 1.2 %fusion.10 = bf16[128,1024]{1,0:T(8,128)(2,1)} fusion(bf16[128,1024]{1,0:T(8,128)(2,1)S(1)} %bitcast.25, bf16[1,1024,1024]{2,1,0:T(8,128)(2,1)S(1)} %copy-done), kind=kOutput, calls=%fused_computation.9 | convolution fusion | flops 268566528 | bytes 2621440 | tf_op jit(solution)/shard_map/dot_general | solution.py:19
  34.1 1.2 %fusion.7 = bf16[128,1024]{1,0:T(8,128)(2,1)} fusion(bf16[128,1024]{1,0:T(8,128)(2,1)S(1)} %bitcast.26, bf16[1,1024,1024]{2,1,0:T(8,128)(2,1)S(1)} %copy-done.1), kind=kOutput, calls=%fused_computation.8 | convolution fusion | flops 268566528 | bytes 2621440 | tf_op jit(solution)/shard_map/dot_general | solution.py:18
  35.3 32.6 %all-reduce.3.cloned.1.call-done = (bf16[128,1024]{1,0:T(8,128)(2,1)}, bf16[128,1024]{1,0:T(8,128)(2,1)}) async-done(((bf16[128,1024]{1,0:T(8,128)(2,1)}, bf16[128,1024]{1,0:T(8,128)(2,1)}), (bf16[128,1024]{1,0:T(8,128)(2,1)}, bf16[128,1024]{1,0:T(8,128)(2,1)})) %all-reduce.3.cloned.1.call-update) | async-done | bytes 524304 | tf_op jit(solution)/shard_map/psum | solution.py:22
  67.9 3.0 %fusion.13 = bf16[128,1024]{1,0:T(8,128)(2,1)} fusion(bf16[1,1024,1024]{2,1,0:T(8,128)(2,1)} %param.18, bf16[128,1024]{1,0:T(8,128)(2,1)} %get-tuple-element.5, bf16[128,1024]{1,0:T(8,128)(2,1)} %get-tuple-element.6), kind=kOutput, calls=%fused_computation.10 | convolution fusion | flops 269615104 | bytes 2883584 | tf_op jit(solution)/shard_map/dot_general | solution.py:25
  70.9 4.6 %all-to-all-start.1 = ((bf16[4,32,1024]{2,1,0:T(8,128)(2,1)}), bf16[4,32,1024]{2,1,0:T(8,128)(2,1)S(1)}, u32[]{:S(2)}, u32[]{:S(2)}) async-start(bf16[4,32,1024]{2,1,0:T(8,128)(2,1)} %bitcast.5), calls=%async_computation.1 | async-start | bytes 524288 | tf_op jit(solution)/shard_map/all_to_all | solution.py:66
  75.6 8.1 %all-to-all-done.1 = bf16[4,32,1024]{2,1,0:T(8,128)(2,1)S(1)} async-done(((bf16[4,32,1024]{2,1,0:T(8,128)(2,1)}), bf16[4,32,1024]{2,1,0:T(8,128)(2,1)S(1)}, u32[]{:S(2)}, u32[]{:S(2)}) %all-to-all-start.1) | async-done | bytes 262176 | tf_op jit(solution)/shard_map/all_to_all | solution.py:66
  83.7 0.3 fusion.6
  84.0 0.1 multiply_reduce_fusion
  84.1 5.7 %psum.31 = f32[64]{0:T(128)S(1)} all-reduce(f32[64]{0:T(128)S(1)} %multiply_reduce_fusion), channel_id=1, replica_groups=mesh['grp'=2,'ep'=4,'tp'=4] {'tp'}, use_global_device_ids=true, to_apply=%region_10.11 | all-reduce | flops 64 | bytes 512 | tf_op jit(solution)/shard_map/psum | solution.py:77
  89.8 0.8 multiply_convert_fusion
  (19 shorter events, 0.2 us)
Async XLA Ops:
  6.5 26.5 %copy-start = (bf16[1,1024,1024]{2,1,0:T(8,128)(2,1)S(1)}, bf16[1,1024,1024]{2,1,0:T(8,128)(2,1)}, u32[]{:S(2)}) copy-start(bf16[1,1024,1024]{2,1,0:T(8,128)(2,1)} %param.17) | copy-start | bytes 6291460
  6.5 61.4 %all-reduce.3.cloned.1.call-start = ((), (), s32[]{:S(2)}) async-start(), calls=%async_computation.2 | async-start | bytes 1048576 | tf_op jit(solution)/shard_map/psum | solution.py:22
  19.1 15.0 %copy-start.1 = (bf16[1,1024,1024]{2,1,0:T(8,128)(2,1)S(1)}, bf16[1,1024,1024]{2,1,0:T(8,128)(2,1)}, u32[]{:S(2)}) copy-start(bf16[1,1024,1024]{2,1,0:T(8,128)(2,1)} %param.16) | copy-start | bytes 6291460
  67.9 7.6 %copy-start.4 = (f32[64,2]{0,1:T(2,128)S(1)}, f32[64,2]{0,1:T(2,128)}, u32[]{:S(2)}) copy-start(f32[64,2]{0,1:T(2,128)} %param.14) | copy-start | bytes 1540
  67.9 7.6 %copy-start.5 = (f32[64]{0:T(128)S(1)}, f32[64]{0:T(128)}, u32[]{:S(2)}) copy-start(f32[64]{0:T(128)} %param.13) | copy-start | bytes 772
  67.9 16.0 %copy-start.2 = (bf16[64,1024]{1,0:T(8,128)(2,1)S(1)}, bf16[64,1024]{1,0:T(8,128)(2,1)}, u32[]{:S(2)}) copy-start(bf16[64,1024]{1,0:T(8,128)(2,1)} %param.10) | copy-start | bytes 393220
  67.9 21.8 %copy-start.3 = (f32[1024]{0:T(1024)S(1)}, f32[1024]{0:T(1024)}, u32[]{:S(2)}) copy-start(f32[1024]{0:T(1024)} %param.19) | copy-start | bytes 12292
  70.9 12.7 %all-to-all-start.1 = ((bf16[4,32,1024]{2,1,0:T(8,128)(2,1)}), bf16[4,32,1024]{2,1,0:T(8,128)(2,1)S(1)}, u32[]{:S(2)}, u32[]{:S(2)}) async-start(bf16[4,32,1024]{2,1,0:T(8,128)(2,1)} %bitcast.5), calls=%async_computation.1 | async-start | bytes 524288 | tf_op jit(solution)/shard_map/all_to_all | solution.py:66
Sparse Core Ops, SparseCore 0:
  35.5 32.4 all-reduce.2
where the time goes:
time: 97.8 us; the launch traced here: 97.4 us
  waiting for transfers between devices  40.7 us (42%)
  blocking collectives  26.5 us (27%)
  between operations  13.5 us (14%)
  matrix products  6.92 us (7%)
  other arithmetic  4.67 us (5%)
  starting transfers between devices  4.6 us (5%)
    psum x1, waiting for transfers between devices, expert_rows(): lax.psum(up_part.astype(jnp.bfloat16), 'tp').astype(jnp.float32)  32.6 us
    all_to_all x1, blocking collectives, local(): lax.all_to_all(outgoing, 'ep', split_axis=0, concat_axis=0, tiled=True)  12.5 us
    psum x1, blocking collectives, local(): square_in = lax.psum(jnp.sum(values * values, axis=1), 'tp')  8.37 us
    all_to_all x1, waiting for transfers between devices, local(): lax.all_to_all(produced.reshape(received.shape), 'ep', split_axis=0, conc...  8.1 us
    psum x1, blocking collectives, local(): square_out = lax.psum(jnp.sum(summed * summed, axis=1), 'tp')  5.66 us
    all_to_all x1, starting transfers between devices, local(): lax.all_to_all(produced.reshape(received.shape), 'ep', split_axis=0, conc...  4.6 us
    dot_general x1, matrix products, expert_rows(): jnp.dot(hidden, down_w, preferred_element_type=jnp.float32)  3 us
  transfers between devices with their start and end apart: 2, of which 2 were waited for; matrix products, arithmetic and copies ran while one was open for 0% of the time, Pallas kernels for 0%

commit v1 on v0

v1 whole, which is shorter than its diff:
```python
import functools

import jax
import jax.numpy as jnp
from jax import lax
from jax.experimental import pallas as pl
from jax.experimental.pallas import tpu as pltpu
from jax.sharding import PartitionSpec as P

EPS = 1e-06
MESH = pl.DeviceIdType.MESH
F32 = jnp.float32
BF16 = jnp.bfloat16


def partner(me, s, n):
    out, bit = me, 1
    while bit < n:
        if s & bit:
            out = out + bit - 2 * bit * ((me // bit) % 2)
        bit *= 2
    return out


def iota(shape, dim):
    return lax.broadcasted_iota(jnp.int32, shape, dim)


def to_row(col, width):
    n = col.shape[0]
    eye = iota((n, width), 0) == iota((n, width), 1)
    return jnp.sum(jnp.where(eye, col, 0.0), axis=0, keepdims=True)


def to_col(row, n):
    width = row.shape[1]
    eye = iota((n, width), 0) == iota((n, width), 1)
    return jnp.sum(jnp.where(eye, row, 0.0), axis=1, keepdims=True)


def kernel(
    cfg,
    x_ref,
    group_ref,
    member_ref,
    prob_ref,
    score_ref,
    ngain_ref,
    wg_hbm,
    wu_hbm,
    wd_hbm,
    fgain_ref,
    out_ref,
    wg,
    wu,
    wd,
    xs,
    xr,
    ps,
    pr,
    sqs,
    sqr,
    hs,
    hr,
    ob,
    ret,
    fs,
    fr,
    w_sem,
    x_send,
    x_recv,
    p_send,
    p_recv,
    q_send,
    q_recv,
    h_send,
    h_recv,
    o_send,
    o_recv,
    f_send,
    f_recv,
):
    n_ep, n_tp, groups, chunks = cfg
    per_group = n_ep // groups
    tok, dim = x_ref.shape
    cap = tok // groups
    ff = wg.shape[1]
    q = ff // n_tp
    full_width = dim * n_tp
    me_e = lax.axis_index("ep")
    me_t = lax.axis_index("tp")

    barrier = pltpu.get_barrier_semaphore()
    for s in range(1, n_ep):
        pl.semaphore_signal(barrier, inc=1, device_id={"ep": partner(me_e, s, n_ep)}, device_id_type=MESH)
    for s in range(1, n_tp):
        pl.semaphore_signal(barrier, inc=1, device_id={"tp": partner(me_t, s, n_tp)}, device_id_type=MESH)

    loads = [
        pltpu.make_async_copy(src.at[0], dst, w_sem.at[i])
        for i, (src, dst) in enumerate(((wg_hbm, wg), (wu_hbm, wu), (wd_hbm, wd)))
    ]
    for load in loads:
        load.start()

    group_row = group_ref[...]
    rows8 = max(8, groups)
    onehot = (iota((rows8, tok), 0) == group_row).astype(F32)
    strict = (iota((tok, tok), 0) < iota((tok, tok), 1)).astype(F32)
    rank = jnp.dot(onehot.astype(BF16), strict.astype(BF16), preferred_element_type=F32)
    slot_row = jnp.sum(
        onehot * (iota((rows8, tok), 0).astype(F32) * cap + rank), axis=0, keepdims=True
    )
    picker = (iota((tok, tok), 0).astype(F32) == slot_row).astype(BF16)
    x = x_ref[...]
    xs[...] = jnp.dot(picker, x, preferred_element_type=F32).astype(BF16)

    pl.semaphore_wait(barrier, n_ep - 1 + n_tp - 1)

    pending = []

    def send(src, dst, ssem, rsem, where):
        copy = pltpu.make_async_remote_copy(
            src_ref=src, dst_ref=dst, send_sem=ssem, recv_sem=rsem, device_id=where, device_id_type=MESH
        )
        copy.start()
        pending.append(copy)
        return copy

    def group_rows(e):
        return pl.ds(pl.multiple_of((e // per_group) * cap, cap), cap)

    x_copies = {}
    for s in range(1, n_ep):
        e = partner(me_e, s, n_ep)
        x_copies[s] = send(
            xs.at[group_rows(e)], xr.at[pl.ds(s * cap, cap)], x_send.at[s], x_recv.at[s], {"ep": e}
        )
    xr[pl.ds(0, cap), :] = xs[group_rows(me_e), :]

    ngain = ngain_ref[...]
    tp_order = [s for s in range(2, n_tp)] + [s for s in range(1, min(2, n_tp))]
    p_copies, q_copies, h_copies, o_copies = {}, {}, {}, {}
    own_parts, own_sq = {}, {}

    def span(c):
        first, count = chunks[c]
        return first * cap, count * cap

    def stage_a(c):
        first, count = chunks[c]
        start, rows = span(c)
        for s in range(first, first + count):
            if s > 0:
                x_copies[s].wait_recv()
        vals = xr[pl.ds(start, rows), :].astype(F32)
        sq = jnp.sum(vals * vals, axis=1, keepdims=True)
        own_sq[c] = sq
        width = sqs.shape[2]
        sqs[c] = jnp.broadcast_to(to_row(sq, width), (8, width))
        for s in tp_order:
            q_copies[c, s] = send(
                sqs.at[c], sqr.at[c, s], q_send.at[c, s], q_recv.at[c, s], {"tp": partner(me_t, s, n_tp)}
            )
        rows_in = (vals * ngain).astype(BF16)
        if c == 0:
            loads[0].wait()
            loads[1].wait()
        for s in tp_order + [0]:
            p = partner(me_t, s, n_tp)
            cols = pl.ds(pl.multiple_of(p * q, q), q)
            g = jnp.dot(rows_in, wg[:, cols], preferred_element_type=F32).astype(BF16)
            u = jnp.dot(rows_in, wu[:, cols], preferred_element_type=F32).astype(BF16)
            if s == 0:
                own_parts[c] = (g, u)
            else:
                ps[s, pl.ds(start, rows), pl.ds(0, q)] = g
                ps[s, pl.ds(start, rows), pl.ds(q, q)] = u
                p_copies[c, s] = send(
                    ps.at[s, pl.ds(start, rows)],
                    pr.at[s, pl.ds(start, rows)],
                    p_send.at[c, s],
                    p_recv.at[c, s],
                    {"tp": p},
                )

    def stage_b(c):
        start, rows = span(c)
        total = own_sq[c]
        for s in range(1, n_tp):
            q_copies[c, s].wait_recv()
            total = total + to_col(sqr[c, s][0:1, :], rows)
        scale = lax.rsqrt(total / full_width + EPS)
        g, u = own_parts[c]
        g, u = g.astype(F32), u.astype(F32)
        for s in range(1, n_tp):
            p_copies[c, s].wait_recv()
            g = g + pr[s, pl.ds(start, rows), pl.ds(0, q)].astype(F32)
            u = u + pr[s, pl.ds(start, rows), pl.ds(q, q)].astype(F32)
        g, u = g * scale, u * scale
        hidden = (g / (1.0 + jnp.exp(-g)) * u).astype(BF16)
        hs[pl.ds(start, rows), :] = hidden
        for s in tp_order:
            h_copies[c, s] = send(
                hs.at[pl.ds(start, rows)],
                hr.at[s, pl.ds(start, rows)],
                h_send.at[c, s],
                h_recv.at[c, s],
                {"tp": partner(me_t, s, n_tp)},
            )

    def stage_c(c):
        first, count = chunks[c]
        start, rows = span(c)
        if c == 0:
            loads[2].wait()
        acc = None
        for s in range(n_tp):
            if s > 0:
                h_copies[c, s].wait_recv()
                h = hr[s, pl.ds(start, rows), :]
            else:
                h = hs[pl.ds(start, rows), :]
            p = partner(me_t, s, n_tp)
            term = jnp.dot(h, wd[pl.ds(pl.multiple_of(p * q, q), q), :], preferred_element_type=F32)
            acc = term if acc is None else acc + term
        ob[pl.ds(start, rows), :] = acc.astype(BF16)
        for s in range(first, first + count):
            if s > 0:
                o_copies[s] = send(
                    ob.at[pl.ds(s * cap, cap)],
                    ret.at[pl.ds(s * cap, cap)],
                    o_send.at[s],
                    o_recv.at[s],
                    {"ep": partner(me_e, s, n_ep)},
                )

    n_chunks = len(chunks)
    for step in range(n_chunks + 4):
        if step < n_chunks:
            stage_a(step)
        if 0 <= step - 1 < n_chunks:
            stage_b(step - 1)
        if 0 <= step - 2 < n_chunks:
            stage_c(step - 2)

    scores = jnp.exp(score_ref[...])
    weights = to_col(prob_ref[...], tok) * scores / jnp.sum(scores, axis=1, keepdims=True)
    slot_col = to_col(slot_row, tok).astype(jnp.int32)
    ids = to_col(group_row.astype(F32), tok).astype(jnp.int32) * per_group + member_ref[...]
    summed = x.astype(F32)
    for s in range(n_ep):
        e = partner(me_e, s, n_ep)
        if s > 0:
            o_copies[s].wait_recv()
            rows = ret[pl.ds(s * cap, cap), :]
        else:
            rows = ob[pl.ds(0, cap), :]
        pick = (iota((tok, cap), 1) + (e // per_group) * cap == slot_col).astype(F32).astype(BF16)
        weight = jnp.sum(jnp.where(ids == e, weights, 0.0), axis=1, keepdims=True)
        summed = summed + weight * jnp.dot(pick, rows, preferred_element_type=F32)

    square = jnp.sum(summed * summed, axis=1, keepdims=True)
    width = fs.shape[1]
    fs[...] = jnp.broadcast_to(to_row(square, width), (8, width))
    f_copies = {}
    for s in tp_order:
        f_copies[s] = send(fs, fr.at[s], f_send.at[s], f_recv.at[s], {"tp": partner(me_t, s, n_tp)})
    for s in range(1, n_tp):
        f_copies[s].wait_recv()
        square = square + to_col(fr[s][0:1, :], tok)
    out_ref[...] = (summed * lax.rsqrt(square / full_width + EPS) * fgain_ref[...]).astype(BF16)

    for copy in pending:
        copy.wait_send()


def solution(mesh):
    n_ep, n_tp = mesh.shape["ep"], mesh.shape["tp"]
    groups = max(2, n_ep // 8)
    n_chunks = 4
    each = n_ep // n_chunks
    chunks = tuple((i * each, each) for i in range(n_chunks))

    def local(tokens, group_choice, member_choice, group_prob, member_score, norm_gain, w_gate, w_up, w_down, final_gain):
        tok, dim = tokens.shape
        ff = w_gate.shape[2]
        cap = tok // groups
        q = ff // n_tp
        all_rows = n_ep * cap
        width = -(-max(count * cap for _, count in chunks) // 128) * 128
        out_width = -(-tok // 128) * 128
        vmem = pl.BlockSpec(memory_space=pltpu.VMEM)
        hbm = pl.BlockSpec(memory_space=pl.ANY)
        dma = pltpu.SemaphoreType.DMA
        nc = len(chunks)
        return pl.pallas_call(
            functools.partial(kernel, (n_ep, n_tp, groups, chunks)),
            out_shape=jax.ShapeDtypeStruct((tok, dim), BF16),
            in_specs=[vmem] * 6 + [hbm] * 3 + [vmem],
            out_specs=vmem,
            scratch_shapes=[
                pltpu.VMEM((dim, ff), BF16),
                pltpu.VMEM((dim, ff), BF16),
                pltpu.VMEM((ff, dim), BF16),
                pltpu.VMEM((tok, dim), BF16),
                pltpu.VMEM((all_rows, dim), BF16),
                pltpu.VMEM((n_tp, all_rows, 2 * q), BF16),
                pltpu.VMEM((n_tp, all_rows, 2 * q), BF16),
                pltpu.VMEM((nc, 8, width), F32),
                pltpu.VMEM((nc, n_tp, 8, width), F32),
                pltpu.VMEM((all_rows, q), BF16),
                pltpu.VMEM((n_tp, all_rows, q), BF16),
                pltpu.VMEM((all_rows, dim), BF16),
                pltpu.VMEM((all_rows, dim), BF16),
                pltpu.VMEM((8, out_width), F32),
                pltpu.VMEM((n_tp, 8, out_width), F32),
                dma((3,)),
                dma((n_ep,)),
                dma((n_ep,)),
                dma((nc, n_tp)),
                dma((nc, n_tp)),
                dma((nc, n_tp)),
                dma((nc, n_tp)),
                dma((nc, n_tp)),
                dma((nc, n_tp)),
                dma((n_ep,)),
                dma((n_ep,)),
                dma((n_tp,)),
                dma((n_tp,)),
            ],
            compiler_params=pltpu.CompilerParams(collective_id=0, has_side_effects=True),
        )(
            tokens,
            group_choice.reshape(1, tok),
            member_choice,
            group_prob.reshape(1, tok),
            member_score,
            norm_gain.reshape(1, dim),
            w_gate,
            w_up,
            w_down,
            final_gain.reshape(1, dim),
        )

    return jax.shard_map(
        local,
        mesh=mesh,
        in_specs=(
            P(("grp", "ep"), "tp"),
            P(("grp", "ep")),
            P(("grp", "ep"), None),
            P(("grp", "ep")),
            P(("grp", "ep"), None),
            P("tp"),
            P("ep", "tp", None),
            P("ep", "tp", None),
            P("ep", None, "tp"),
            P("tp"),
        ),
        out_specs=P(("grp", "ep"), "tp"),
        check_vma=False,
    )
```

time: 97.8 us -> 35.1 us (0.36)
  waiting for transfers between devices: 40.7 us -> 0 us
  Pallas kernels: 0 us -> 30.6 us
  blocking collectives: 26.5 us -> 0 us
  between operations: 13.5 us -> 0.01 us
  matrix products: 6.92 us -> 0 us
  other arithmetic: 4.67 us -> 0 us
  starting transfers between devices: 4.6 us -> 0 us
  local copies, waits for them, and re-layouts: 0.47 us -> 4.31 us
    psum x1 -> x0, waiting for transfers between devices: 32.6 us -> none  [expert_rows(): lax.psum(up_part.astype(jnp.bfloat16), 'tp').astype(jnp.float32)]
    pallas_call x0 -> x1, Pallas kernels: none -> 30.6 us  [local(): pl.pallas_call(functools.partial(kernel, (n_ep, n_tp, groups, chunks)), o...]
    psum x2 -> x0, blocking collectives: 14 us -> none  [the longest x1 8.37 us: local(): square_in = lax.psum(jnp.sum(values * values, axis=1), 'tp')]
    all_to_all x1 -> x0, blocking collectives: 12.5 us -> none  [local(): lax.all_to_all(outgoing, 'ep', split_axis=0, concat_axis=0, tiled=True)]
    all_to_all x1 -> x0, waiting for transfers between devices: 8.1 us -> none  [local(): lax.all_to_all(produced.reshape(received.shape), 'ep', split_axis=0, conc...]
    dot_general x5 -> x0, matrix products: 6.92 us -> none  [the longest x1 3 us: expert_rows(): jnp.dot(hidden, down_w, preferred_element_type=jnp.float32)]
    all_to_all x1 -> x0, starting transfers between devices: 4.6 us -> none  [local(): lax.all_to_all(produced.reshape(received.shape), 'ep', split_axis=0, conc...]
    unnamed x12 -> x3, local copies, waits for them, and re-layouts: 0.02 us -> 4.31 us
  transfers between devices with their start and end apart: 2 -> 0, of which waited for: 2 -> 0; matrix products, arithmetic and copies ran while one was open for 0% -> 0% of each run, Pallas kernels for 0% -> 0%
where the time goes in v1:
time: 35.1 us; the launch traced here: 34.9 us
  Pallas kernels  30.6 us (87%)
  local copies, waits for them, and re-layouts  4.31 us (12%)
    pallas_call x1, Pallas kernels, local(): pl.pallas_call(functools.partial(kernel, (n_ep, n_tp, groups, chunks)), o...  30.6 us
    unnamed x3, local copies, waits for them, and re-layouts  4.31 us

profile of v1, /device:TPU:0, one launch (start us, length us, event | category | flops | bytes accessed | tf_op | source)
XLA Modules:
  0.0 34.9 jit_solution(10359877737371646049)
XLA Ops:
  0.0 1.4 %copy.11.member_ref = s32[64,2]{1,0:T(8,128)} copy(s32[64,2]{0,1:T(2,128)} %param.12) | data formatting | bytes 1024 | tf_op args[2]
  1.4 1.4 %copy.12.score_ref = f32[64,2]{1,0:T(8,128)} copy(f32[64,2]{0,1:T(2,128)} %param.14) | data formatting | bytes 1024 | tf_op args[4]
  2.7 30.6 %shard_map.100 = bf16[64,1024]{1,0:T(8,128)(2,1)} custom-call(bf16[64,1024]{1,0:T(8,128)(2,1)} %x_ref.1, s32[1,64]{1,0:T(1,128)} %bitcast.6, s32[64,2]{1,0:T(8,128)} %copy.11.member_ref, f32[1,64]{1,0:T(1,128)} %bitcast.7, f32[64,2]{1,0:T(8,128)} %copy.12.score_ref, f32[1,1024]{1,0:T(1,128)} %bitcast.4, bf16[1,1024,1024]{2,1,0:T(8,128)(2,1)} %wg_hbm.1, ...), custom_call_target="tpu_custom_call" | custom-call | tf_op jit(solution)/shard_map/pallas_call | solution.py:297
  33.3 1.6 %copy.14 = bf16[64,1024]{1,0:T(8,128)(2,1)} copy(bf16[64,1024]{1,0:T(8,128)(2,1)} %shard_map.100) | data formatting | bytes 262144

commit v2 on v1

v2 whole, which is shorter than its diff:
```python
import functools

import jax
import jax.numpy as jnp
from jax import lax
from jax.experimental import pallas as pl
from jax.experimental.pallas import tpu as pltpu
from jax.sharding import PartitionSpec as P

EPS = 1e-06
MESH = pl.DeviceIdType.MESH
F32 = jnp.float32
BF16 = jnp.bfloat16
PLAN = (
    ("a", 0), ("a", 1), ("b", 0), ("a", 2), ("a", 3), ("b", 1),
    ("c", 0), ("b", 2), ("b", 3), ("c", 1), ("c", 2), ("c", 3),
)
VMEM_LIMIT = 60 * 2**20


def partner(me, s, n):
    out, bit = me, 1
    while bit < n:
        if s & bit:
            out = out + bit - 2 * bit * ((me // bit) % 2)
        bit *= 2
    return out


def iota(shape, dim):
    return lax.broadcasted_iota(jnp.int32, shape, dim)


def to_row(col, width):
    n = col.shape[0]
    eye = iota((n, width), 0) == iota((n, width), 1)
    return jnp.sum(jnp.where(eye, col, 0.0), axis=0, keepdims=True)


def to_col(row, n):
    width = row.shape[1]
    eye = iota((n, width), 0) == iota((n, width), 1)
    return jnp.sum(jnp.where(eye, row, 0.0), axis=1, keepdims=True)


def kernel(
    cfg,
    x_hbm,
    group_hbm,
    member_hbm,
    prob_hbm,
    score_hbm,
    ngain_hbm,
    wg_hbm,
    wu_hbm,
    wd_hbm,
    out_ref,
    x_ref,
    group_ref,
    member_ref,
    prob_ref,
    score_ref,
    ngain_ref,
    wg,
    wu,
    wd,
    xs,
    xr,
    ps,
    pr,
    sqs,
    sqr,
    hs,
    hr,
    ob,
    ret,
    fs,
    fr,
    w_sem,
    x_send,
    x_recv,
    p_send,
    p_recv,
    q_send,
    q_recv,
    h_send,
    h_recv,
    o_send,
    o_recv,
    f_send,
    f_recv,
):
    n_ep, n_tp, groups, order, chunks = cfg
    per_group = n_ep // groups
    tok, dim = x_ref.shape
    cap = tok // groups
    ff = wg.shape[1]
    q = ff // n_tp
    full_width = dim * n_tp
    me_e = lax.axis_index("ep")
    me_t = lax.axis_index("tp")

    barrier = pltpu.get_barrier_semaphore()
    for s in range(1, n_ep):
        pl.semaphore_signal(barrier, inc=1, device_id={"ep": partner(me_e, s, n_ep)}, device_id_type=MESH)
    for s in range(1, n_tp):
        pl.semaphore_signal(barrier, inc=1, device_id={"tp": partner(me_t, s, n_tp)}, device_id_type=MESH)

    moves = (
        (group_hbm, group_ref),
        (x_hbm, x_ref),
        (ngain_hbm, ngain_ref),
        (wg_hbm.at[0], wg),
        (wu_hbm.at[0], wu),
        (member_hbm, member_ref),
        (prob_hbm, prob_ref),
        (score_hbm, score_ref),
        (wd_hbm.at[0], wd),
    )
    loads = [pltpu.make_async_copy(src, dst, w_sem.at[i]) for i, (src, dst) in enumerate(moves)]
    for load in loads:
        load.start()
    loads[0].wait()
    loads[1].wait()

    group_row = group_ref[...]
    rows8 = max(8, groups)
    onehot = (iota((rows8, tok), 0) == group_row).astype(F32)
    strict = (iota((tok, tok), 0) < iota((tok, tok), 1)).astype(F32)
    rank = jnp.dot(onehot.astype(BF16), strict.astype(BF16), preferred_element_type=F32)
    slot_row = jnp.sum(
        onehot * (iota((rows8, tok), 0).astype(F32) * cap + rank), axis=0, keepdims=True
    )
    picker = (iota((tok, tok), 0).astype(F32) == slot_row).astype(BF16)
    x = x_ref[...]
    xs[...] = jnp.dot(picker, x, preferred_element_type=F32).astype(BF16)

    pending = []

    def send(src, dst, ssem, rsem, where):
        copy = pltpu.make_async_remote_copy(
            src_ref=src, dst_ref=dst, send_sem=ssem, recv_sem=rsem, device_id=where, device_id_type=MESH
        )
        copy.start()
        pending.append(copy)
        return copy

    def group_rows(e):
        return pl.ds(pl.multiple_of((e // per_group) * cap, cap), cap)

    xr[pl.ds(0, cap), :] = xs[group_rows(me_e), :]
    x_copies = {}

    def dispatch():
        for k in range(1, n_ep):
            e = partner(me_e, order[k], n_ep)
            x_copies[k] = send(
                xs.at[group_rows(e)], xr.at[pl.ds(k * cap, cap)], x_send.at[k], x_recv.at[k], {"ep": e}
            )

    loads[2].wait()
    ngain = ngain_ref[...]
    tp_order = [s for s in range(2, n_tp)] + [s for s in range(1, min(2, n_tp))]
    p_copies, q_copies, h_copies, o_copies = {}, {}, {}, {}
    own_sq = {}

    def span(c):
        first, count = chunks[c]
        return first * cap, count * cap

    def products(c):
        start, rows = span(c)
        vals = xr[pl.ds(start, rows), :].astype(F32)
        sq = jnp.sum(vals * vals, axis=1, keepdims=True)
        own_sq[c] = sq
        width = sqs.shape[2]
        sqs[c] = jnp.broadcast_to(to_row(sq, width), (8, width))
        rows_in = (vals * ngain).astype(BF16)
        for s in tp_order + [0]:
            p = partner(me_t, s, n_tp)
            cols = pl.ds(pl.multiple_of(p * q, q), q)
            ps[s, pl.ds(start, rows), pl.ds(0, q)] = jnp.dot(
                rows_in, wg[:, cols], preferred_element_type=F32
            ).astype(BF16)
            ps[s, pl.ds(start, rows), pl.ds(q, q)] = jnp.dot(
                rows_in, wu[:, cols], preferred_element_type=F32
            ).astype(BF16)
            if s > 0:
                send_part(c, s)

    def send_part(c, s):
        start, rows = span(c)
        peer = {"tp": partner(me_t, s, n_tp)}
        p_copies[c, s] = send(
            ps.at[s, pl.ds(start, rows)],
            pr.at[s, pl.ds(start, rows)],
            p_send.at[c, s],
            p_recv.at[c, s],
            peer,
        )
        q_copies[c, s] = send(sqs.at[c], sqr.at[c, s], q_send.at[c, s], q_recv.at[c, s], peer)

    def stage_a(c):
        first, count = chunks[c]
        for k in range(max(first, 1), first + count):
            x_copies[k].wait_recv()
        products(c)

    def stage_b(c):
        start, rows = span(c)
        total = own_sq[c]
        for s in range(1, n_tp):
            q_copies[c, s].wait_recv()
            total = total + to_col(sqr[c, s][0:1, :], rows)
        scale = lax.rsqrt(total / full_width + EPS)
        g = ps[0, pl.ds(start, rows), pl.ds(0, q)].astype(F32)
        u = ps[0, pl.ds(start, rows), pl.ds(q, q)].astype(F32)
        for s in range(1, n_tp):
            p_copies[c, s].wait_recv()
            g = g + pr[s, pl.ds(start, rows), pl.ds(0, q)].astype(F32)
            u = u + pr[s, pl.ds(start, rows), pl.ds(q, q)].astype(F32)
        g, u = g * scale, u * scale
        hidden = (g / (1.0 + jnp.exp(-g)) * u).astype(BF16)
        hs[pl.ds(start, rows), :] = hidden
        for s in tp_order:
            h_copies[c, s] = send(
                hs.at[pl.ds(start, rows)],
                hr.at[s, pl.ds(start, rows)],
                h_send.at[c, s],
                h_recv.at[c, s],
                {"tp": partner(me_t, s, n_tp)},
            )

    def stage_c(c):
        first, count = chunks[c]
        start, rows = span(c)
        if c == 0:
            loads[8].wait()
        acc = None
        for s in range(n_tp):
            if s > 0:
                h_copies[c, s].wait_recv()
                h = hr[s, pl.ds(start, rows), :]
            else:
                h = hs[pl.ds(start, rows), :]
            p = partner(me_t, s, n_tp)
            term = jnp.dot(h, wd[pl.ds(pl.multiple_of(p * q, q), q), :], preferred_element_type=F32)
            acc = term if acc is None else acc + term
        ob[pl.ds(start, rows), :] = acc.astype(BF16)
        for k in range(first, first + count):
            if k > 0:
                o_copies[k] = send(
                    ob.at[pl.ds(k * cap, cap)],
                    ret.at[pl.ds(k * cap, cap)],
                    o_send.at[k],
                    o_recv.at[k],
                    {"ep": partner(me_e, order[k], n_ep)},
                )

    pl.semaphore_wait(barrier, n_ep - 1 + n_tp - 1)
    dispatch()
    loads[3].wait()
    loads[4].wait()
    stage_a(0)
    for load in loads[5:8]:
        load.wait()
    scores = jnp.exp(score_ref[...])
    weights = prob_ref[...] * scores / jnp.sum(scores, axis=0, keepdims=True)
    slot_col = to_col(slot_row, tok).astype(jnp.int32)
    ids = group_row * per_group + member_ref[...]
    expert_cols = []
    for k in range(n_ep):
        named = jnp.where(ids == partner(me_e, order[k], n_ep), weights, 0.0)
        expert_cols.append(to_col(jnp.sum(named, axis=0, keepdims=True), tok))

    stages = {"a": stage_a, "b": stage_b, "c": stage_c}
    for stage, c in PLAN[1:]:
        stages[stage](c)

    summed = x.astype(F32)
    for k in range(n_ep):
        e = partner(me_e, order[k], n_ep)
        if k > 0:
            o_copies[k].wait_recv()
            rows = ret[pl.ds(k * cap, cap), :]
        else:
            rows = ob[pl.ds(0, cap), :]
        pick = (iota((tok, cap), 1) + (e // per_group) * cap == slot_col).astype(F32).astype(BF16)
        summed = summed + expert_cols[k] * jnp.dot(pick, rows, preferred_element_type=F32)

    square = jnp.sum(summed * summed, axis=1, keepdims=True)
    width = fs.shape[1]
    fs[...] = jnp.broadcast_to(to_row(square, width), (8, width))
    f_copies = {}
    for s in tp_order:
        f_copies[s] = send(fs, fr.at[s], f_send.at[s], f_recv.at[s], {"tp": partner(me_t, s, n_tp)})
    for s in range(1, n_tp):
        f_copies[s].wait_recv()
        square = square + to_col(fr[s][0:1, :], tok)
    out_ref[...] = summed * lax.rsqrt(square / full_width + EPS)

    for copy in pending:
        copy.wait_send()


def solution(mesh):
    n_ep, n_tp = mesh.shape["ep"], mesh.shape["tp"]
    groups = max(2, n_ep // 8)
    order = range(n_ep)
    n_chunks = 4
    each = n_ep // n_chunks
    chunks = tuple((i * each, each) for i in range(n_chunks))

    def local(tokens, group_choice, member_choice, group_prob, member_score, norm_gain, w_gate, w_up, w_down, final_gain):
        tok, dim = tokens.shape
        ff, top = w_gate.shape[2], member_choice.shape[1]
        cap = tok // groups
        q = ff // n_tp
        all_rows = n_ep * cap
        width = -(-max(count * cap for _, count in chunks) // 128) * 128
        out_width = -(-tok // 128) * 128
        vmem = pl.BlockSpec(memory_space=pltpu.VMEM)
        hbm = pl.BlockSpec(memory_space=pltpu.HBM)
        dma = pltpu.SemaphoreType.DMA
        nc = len(chunks)
        normal = pl.pallas_call(
            functools.partial(kernel, (n_ep, n_tp, groups, tuple(order), chunks)),
            out_shape=jax.ShapeDtypeStruct((tok, dim), F32),
            in_specs=[hbm] * 9,
            out_specs=vmem,
            scratch_shapes=[
                pltpu.VMEM((tok, dim), BF16),
                pltpu.VMEM((1, tok), jnp.int32),
                pltpu.VMEM((top, tok), jnp.int32),
                pltpu.VMEM((1, tok), F32),
                pltpu.VMEM((top, tok), F32),
                pltpu.VMEM((1, dim), F32),
                pltpu.VMEM((dim, ff), BF16),
                pltpu.VMEM((dim, ff), BF16),
                pltpu.VMEM((ff, dim), BF16),
                pltpu.VMEM((tok, dim), BF16),
                pltpu.VMEM((all_rows, dim), BF16),
                pltpu.VMEM((n_tp, all_rows, 2 * q), BF16),
                pltpu.VMEM((n_tp, all_rows, 2 * q), BF16),
                pltpu.VMEM((nc, 8, width), F32),
                pltpu.VMEM((nc, n_tp, 8, width), F32),
                pltpu.VMEM((all_rows, q), BF16),
                pltpu.VMEM((n_tp, all_rows, q), BF16),
                pltpu.VMEM((all_rows, dim), BF16),
                pltpu.VMEM((all_rows, dim), BF16),
                pltpu.VMEM((8, out_width), F32),
                pltpu.VMEM((n_tp, 8, out_width), F32),
                dma((9,)),
                dma((n_ep,)),
                dma((n_ep,)),
                dma((nc, n_tp)),
                dma((nc, n_tp)),
                dma((nc, n_tp)),
                dma((nc, n_tp)),
                dma((nc, n_tp)),
                dma((nc, n_tp)),
                dma((n_ep,)),
                dma((n_ep,)),
                dma((n_tp,)),
                dma((n_tp,)),
            ],
            compiler_params=pltpu.CompilerParams(collective_id=0, has_side_effects=True, vmem_limit_bytes=VMEM_LIMIT),
        )(
            tokens,
            group_choice.reshape(1, tok),
            member_choice.T,
            group_prob.reshape(1, tok),
            member_score.T,
            norm_gain.reshape(1, dim),
            w_gate,
            w_up,
            w_down,
        )
        return (normal * final_gain[None, :]).astype(BF16)

    return jax.shard_map(
        local,
        mesh=mesh,
        in_specs=(
            P(("grp", "ep"), "tp"),
            P(("grp", "ep")),
            P(("grp", "ep"), None),
            P(("grp", "ep")),
            P(("grp", "ep"), None),
            P("tp"),
            P("ep", "tp", None),
            P("ep", "tp", None),
            P("ep", None, "tp"),
            P("tp"),
        ),
        out_specs=P(("grp", "ep"), "tp"),
        check_vma=False,
    )
```

time: 35.1 us -> 31.1 us (0.89)
  local copies, waits for them, and re-layouts: 4.31 us -> 0.01 us
  other arithmetic: 0 us -> 1.62 us
  Pallas kernels: 30.6 us -> 29.3 us
    unnamed x3 -> x2, local copies, waits for them, and re-layouts: 4.31 us -> 0.01 us
    convert_element_type x0 -> x1, other arithmetic: none -> 1.62 us  [local(): return (normal * final_gain[None, :]).astype(BF16)]
    pallas_call x1, Pallas kernels: 30.6 us -> 29.3 us  [local(): pl.pallas_call(functools.partial(kernel, (n_ep, n_tp, groups, tuple(order...]
where the time goes in v2:
time: 31.1 us; the launch traced here: 30.9 us
  Pallas kernels  29.3 us (94%)
  other arithmetic  1.62 us (5%)
    pallas_call x1, Pallas kernels, local(): pl.pallas_call(functools.partial(kernel, (n_ep, n_tp, groups, tuple(order...  29.3 us
    convert_element_type x1, other arithmetic, local(): return (normal * final_gain[None, :]).astype(BF16)  1.62 us

profile of v2, /device:TPU:0, one launch (start us, length us, event | category | flops | bytes accessed | tf_op | source)
XLA Modules:
  0.0 30.9 jit_solution(1674276682462401710)
XLA Ops:
  0.0 0.0 copy-start
  0.0 29.3 %shard_map.100 = f32[64,1024]{1,0:T(8,128)} custom-call(bf16[64,1024]{1,0:T(8,128)(2,1)} %x_hbm.1, s32[1,64]{1,0:T(1,128)} %bitcast.8, s32[2,64]{1,0:T(2,128)} %bitcast.6, f32[1,64]{1,0:T(1,128)} %bitcast.9, f32[2,64]{1,0:T(2,128)} %bitcast.7, f32[1,1024]{1,0:T(1,128)} %bitcast.5, bf16[1,1024,1024]{2,1,0:T(8,128)(2,1)} %wg_hbm.1, ...), custom_call_target="tpu_custom_call" | custom-call | tf_op jit(solution)/shard_map/pallas_call | solution.py:326
  29.3 0.0 copy-done
  29.3 1.6 %multiply_convert_fusion = bf16[64,1024]{1,0:T(8,128)(2,1)} fusion(f32[64,1024]{1,0:T(8,128)} %shard_map.100, f32[1024]{0:T(1024)S(1)} %copy-done), kind=kLoop, calls=%fused_computation | loop fusion | flops 131072 | bytes 397312 | tf_op jit(solution)/shard_map/convert_element_type | solution.py:379
Async XLA Ops:
  0.0 29.3 %copy-start = (f32[1024]{0:T(1024)S(1)}, f32[1024]{0:T(1024)}, u32[]{:S(2)}) copy-start(f32[1024]{0:T(1024)} %param.19) | copy-start | bytes 12292

commit v3 on v2

--- a/solution.py
+++ b/solution.py
@@ -13,9 +13,9 @@
 BF16 = jnp.bfloat16
 PLAN = (
     ("a", 0), ("a", 1), ("b", 0), ("a", 2), ("a", 3), ("b", 1),
-    ("c", 0), ("b", 2), ("b", 3), ("c", 1), ("c", 2), ("c", 3),
+    ("c", 0), ("b", 2), ("b", 3), ("c", 2), ("c", 1), ("c", 3),
 )
-VMEM_LIMIT = 60 * 2**20
+VMEM_LIMIT = 56 * 2**20
 
 
 def partner(me, s, n):
@@ -325,7 +325,7 @@
         nc = len(chunks)
         normal = pl.pallas_call(
             functools.partial(kernel, (n_ep, n_tp, groups, tuple(order), chunks)),
-            out_shape=jax.ShapeDtypeStruct((tok, dim), F32),
+            out_shape=pltpu.VMEM((tok, dim), F32),
             in_specs=[hbm] * 9,
             out_specs=vmem,
             scratch_shapes=[

time: 31.1 us -> 30.3 us (0.974)
  other arithmetic: 1.62 us -> 0.67 us
    convert_element_type x1, other arithmetic: 1.62 us -> 0.67 us  [local(): return (normal * final_gain[None, :]).astype(BF16)]
where the time goes in v3:
time: 30.3 us; the launch traced here: 30.1 us
  Pallas kernels  29.4 us (97%)
  other arithmetic  0.67 us (2%)
    pallas_call x1, Pallas kernels, local(): pl.pallas_call(functools.partial(kernel, (n_ep, n_tp, groups, tuple(order...  29.4 us
    convert_element_type x1, other arithmetic, local(): return (normal * final_gain[None, :]).astype(BF16)  0.67 us

profile of v3, /device:TPU:0, one launch (start us, length us, event | category | flops | bytes accessed | tf_op | source)
XLA Modules:
  0.0 30.1 jit_solution(14172527165361611998)
XLA Ops:
  0.0 0.0 copy-start
  0.0 29.4 %shard_map.100 = f32[64,1024]{1,0:T(8,128)S(1)} custom-call(bf16[64,1024]{1,0:T(8,128)(2,1)} %x_hbm.1, s32[1,64]{1,0:T(1,128)} %bitcast.8, s32[2,64]{1,0:T(2,128)} %bitcast.6, f32[1,64]{1,0:T(1,128)} %bitcast.9, f32[2,64]{1,0:T(2,128)} %bitcast.7, f32[1,1024]{1,0:T(1,128)} %bitcast.5, bf16[1,1024,1024]{2,1,0:T(8,128)(2,1)} %wg_hbm.1, ...), custom_call_target="tpu_custom_call" | custom-call | tf_op jit(solution)/shard_map/pallas_call | solution.py:326
  29.4 0.0 copy-done
  29.4 0.7 %multiply_convert_fusion = bf16[64,1024]{1,0:T(8,128)(2,1)} fusion(f32[64,1024]{1,0:T(8,128)S(1)} %shard_map.100, f32[1024]{0:T(1024)S(1)} %copy-done), kind=kLoop, calls=%fused_computation | loop fusion | flops 131072 | bytes 397312 | tf_op jit(solution)/shard_map/convert_element_type | solution.py:379
Async XLA Ops:
  0.0 29.4 %copy-start = (f32[1024]{0:T(1024)S(1)}, f32[1024]{0:T(1024)}, u32[]{:S(2)}) copy-start(f32[1024]{0:T(1024)} %param.19) | copy-start | bytes 12292
